TPU v7x, 256 devices: a 4x2x16 block of a 4x16x16 slice. The times are simulated.
256 devices in a mesh: grp: 2 (over y), sp: 16 (over z), tp: 4 (over x), dp: 2 (over core).
Axes of the slice: x: 4, y: 2, z: 16, core: 2. Of those that a mesh axis runs over, the one named last changes fastest.
The devices are a block of a 4x16x16 slice.
Arguments:
- latent: bfloat16 [24576, 4096], P(('grp', 'sp', 'dp')), parts along dimension 0, may hold values from -6 to 6
- context: bfloat16 [1024, 4096], P(('grp', 'sp')), parts along dimension 0, may hold values from -6 to 6
- condition: bfloat16 [8192], P('grp'), parts along dimension 0, may hold values from -6 to 6
- context_condition: bfloat16 [4096], replicated, may hold values from -6 to 6
- shift_weight: bfloat16 [4096, 4096], P('sp', ('tp', 'dp')), may hold values from -0.09375 to 0.09375
- scale_weight: bfloat16 [4096, 4096], P('sp', ('tp', 'dp')), may hold values from -0.09375 to 0.09375
- gate_weight: bfloat16 [4096, 4096], P('sp', ('tp', 'dp')), may hold values from -0.09375 to 0.09375
- norm_gain: float32 [4096], replicated, may hold values from 0.1 to 1.9
- out_gate_weight: bfloat16 [4096, 2048], P(None, ('tp', 'dp')), may hold values from -0.09375 to 0.09375
- signal_weight: bfloat16 [4096, 2048], P(None, ('tp', 'dp')), may hold values from -0.09375 to 0.09375
- writer_weight: bfloat16 [4096, 1024], P(None, ('tp', 'dp')), may hold values from -0.09375 to 0.09375
- reader_matrix: bfloat16 [4096, 1024], P(None, ('tp', 'dp')), may hold values from -0.09375 to 0.09375
- step_weight: bfloat16 [2, 4096, 32], P(None, None, ('tp', 'dp')), may hold values from -0.09375 to 0.09375
- signal_taps: float32 [3, 2048], P(None, ('tp', 'dp')), may hold values from -3.5 to 3.5
- writer_taps: float32 [3, 1024], P(None, ('tp', 'dp')), may hold values from -3.5 to 3.5
- reader_taps: float32 [3, 1024], P(None, ('tp', 'dp')), may hold values from -3.5 to 3.5
- step_bias: float32 [2, 32], P(None, ('tp', 'dp')), may hold values from -4.5 to -2.5
- decay_log: float32 [2, 32], P(None, ('tp', 'dp')), may hold values from -12 to 1
- decay_extra: float32 [2, 32, 24576], P(None, ('tp', 'dp'), ('grp', 'sp')), parts along dimension 2, may hold values from -3 to 0
- group_gain: float32 [2048], P(('tp', 'dp')), may hold values from 0.1 to 1.9
- output_weight: bfloat16 [2048, 4096], P(None, ('tp', 'dp')), may hold values from -0.125 to 0.125
Outputs:
- updated: bfloat16 [24576, 4096], P(('grp', 'sp'), ('tp', 'dp')), parts along dimension 0
There are 2 independent parts, one for each index of `grp`. A program takes and returns all parts, laid end to end along the dimension named above; an argument that names none is the same for every part. Nothing has to cross between parts.
All inputs are finite; a program needn't handle non-finite values.
Results may differ from a plain program's by a relative error of at most 0.007.
Values may be sent and summed in bfloat16 or wider, within the bound.
No kernel may reach another device: no remote copies, remote signals or barrier semaphores. Data moves between devices by JAX's collectives and lax.ppermute only.
A program may use at most 128 MiB of HBM per device.

v0:
```python
import jax
import jax.numpy as jnp
from jax import lax
from jax.sharding import PartitionSpec as P

STATE = 128
BLOCK = 128
EPSILON = 1e-06


def copy_for_each(x, axis):
    copies = jnp.broadcast_to(x, (lax.axis_size(axis), *x.shape))
    return lax.all_to_all(copies, axis, split_axis=0, concat_axis=0, tiled=True)


def of_everyone(x, axis):
    everything = copy_for_each(x, axis)
    return jnp.sum(everything, axis=0)


def in_one(arrays, axis):
    ends = [0]
    for a in arrays:
        ends.append(ends[-1] + a.size)
    subtotal = of_everyone(jnp.concatenate([a.ravel() for a in arrays]), axis)
    return tuple((subtotal[b:e].reshape(a.shape) for a, b, e in zip(arrays, ends, ends[1:])))


def side_by_side(arrays, axis, dim, along):
    ends, at = ([], 0)
    for a in arrays[:-1]:
        at += a.shape[along]
        ends.append(at)
    both = jnp.concatenate(arrays, axis=along)
    return tuple(jnp.split(lax.all_gather(both, axis, axis=dim, tiled=True), ends, axis=along))


def rows_first(arrays, axis, dims):
    turned = [jnp.moveaxis(a, dim, 0) for a, dim in zip(arrays, dims)]
    widths = [t[0].size for t in turned]
    both = jnp.concatenate([t.reshape(-1, w) for t, w in zip(turned, widths)], axis=1)
    out = lax.all_gather(both, axis, axis=0, tiled=True)
    tiles = jnp.split(out, [sum(widths[:k]) for k in range(1, len(widths))], axis=1)
    return tuple(
        (
            jnp.moveaxis(b.reshape(-1, *t.shape[1:]), 0, dim)
            for b, t, dim in zip(tiles, turned, dims)
        )
    )


def extended(cells, sides, width):
    for axis, dim in sides:
        count = lax.axis_size(axis)
        ends = count - 1
        head = lax.slice_in_dim(cells, 0, width, axis=dim)
        tail = lax.slice_in_dim(cells, cells.shape[dim] - width, cells.shape[dim], axis=dim)
        cells = jnp.concatenate(
            [
                lax.ppermute(tail, axis, [(i, (i + 1) % count) for i in range(ends)]),
                cells,
                lax.ppermute(head, axis, [((i + 1) % count, i) for i in range(ends)]),
            ],
            axis=dim,
        )
    return cells


def entering(x, axis, combine, identity, reverse):
    devices, position = (lax.axis_size(axis), lax.axis_index(axis))
    everything = jax.tree.map(lambda part: lax.all_gather(part, axis), x)
    start = jax.tree.map(
        lambda part, zero: jnp.broadcast_to(jnp.asarray(zero, part.dtype), part.shape), x, identity
    )

    def turn(k, before):
        at = devices - 1 - k if reverse else k
        reached = at > position if reverse else at < position
        new = combine(before, jax.tree.map(lambda part: part[at], everything))
        return jax.tree.map(lambda a, b: jnp.where(reached, a, b), new, before)

    return lax.fori_loop(0, devices, turn, start)


def modulate(rows, norm_gain, shift_vec, scale_vec):
    values = rows.astype(jnp.float32)
    normed = (
        values * lax.rsqrt(jnp.mean(values * values, axis=-1, keepdims=True) + EPSILON) * norm_gain
    )
    return (normed * (1.0 + scale_vec) + shift_vec).astype(jnp.bfloat16)


def centred_conv(padded, conv_taps, length):
    running = jnp.zeros((length, padded.shape[1]), jnp.float32)
    for offset in range(conv_taps.shape[0]):
        running = running + conv_taps[offset] * padded[offset : offset + length].astype(jnp.float32)
    return jax.nn.silu(running)


def project_rows(hidden, signal_weight, writer_weight, reader_matrix, step_weight):
    raw_cols = jnp.concatenate(
        [
            jnp.dot(hidden, signal_weight, preferred_element_type=jnp.float32),
            jnp.dot(hidden, writer_weight, preferred_element_type=jnp.float32),
            jnp.dot(hidden, reader_matrix, preferred_element_type=jnp.float32),
        ],
        axis=1,
    ).astype(jnp.bfloat16)
    step_in = jnp.stack(
        [
            jnp.dot(hidden, step_weight[0], preferred_element_type=jnp.float32),
            jnp.dot(hidden, step_weight[1], preferred_element_type=jnp.float32),
        ]
    ).astype(jnp.bfloat16)
    return (raw_cols, step_in)


def split_mixed(conv_out, head_count, head_width, group_count, state_width):
    length = conv_out.shape[0]
    signal_end = head_count * head_width
    writer_end = signal_end + group_count * state_width
    signal = conv_out[:, :signal_end].reshape(length, head_count, head_width)
    writer = conv_out[:, signal_end:writer_end].reshape(length, group_count, state_width)
    reader = conv_out[:, writer_end:].reshape(length, group_count, state_width)
    return (signal, writer, reader)


def state_span(signal, step_size, log_decay, writer, reader, start_state, block):
    length, head_count, head_width = signal.shape
    group_count, state_width = (writer.shape[1], writer.shape[2])
    per_group = head_count // group_count
    blocks = length // block
    scaled = (signal * step_size[..., None]).reshape(
        blocks, block, group_count, per_group, head_width
    )
    cum_log = jnp.cumsum(log_decay.reshape(blocks, block, group_count, per_group), axis=1)
    writer_blk = writer.reshape(blocks, block, group_count, state_width)
    reader_blk = reader.reshape(blocks, block, group_count, state_width)
    inner_dot = jnp.einsum("bign,bjgn->bgij", reader_blk, writer_blk)
    moved = jnp.moveaxis(cum_log, 1, -1)
    gap_logs = moved[..., :, None] - moved[..., None, :]
    lower_mask = jnp.tril(jnp.ones((block, block), dtype=bool))
    weights = jnp.exp(jnp.where(lower_mask, gap_logs, -jnp.inf))
    in_block = jnp.einsum("bgij,bgeij,bjgep->bigep", inner_dot, weights, scaled)
    to_end = jnp.exp(cum_log[:, -1:] - cum_log)
    states = jnp.einsum("bjgn,bjge,bjgep->bgepn", writer_blk, to_end, scaled)
    block_decay = jnp.exp(cum_log[:, -1])

    def advance(running, block_item):
        state_add, decay_now = block_item
        return (running * decay_now[..., None, None] + state_add, running)

    last_state, before = lax.scan(
        advance,
        start_state.reshape(group_count, per_group, head_width, state_width),
        (states, block_decay),
    )
    carried = jnp.einsum("bign,bgepn,bige->bigep", reader_blk, before, jnp.exp(cum_log))
    result = (in_block + carried).reshape(length, head_count, head_width)
    return (result, last_state.reshape(head_count, head_width, state_width))


def context_state(signal, row_weights, writer):
    length, head_count, head_width = signal.shape
    group_count, state_width = (writer.shape[1], writer.shape[2])
    per_group = head_count // group_count
    grouped = signal.reshape(length, group_count, per_group, head_width)
    weights = row_weights.reshape(length, group_count, per_group)
    summed = jnp.einsum("tgn,tge,tgep->gepn", writer, weights, grouped)
    return summed.reshape(head_count, head_width, state_width)


def group_norm(gated, group_count, group_gain):
    length = gated.shape[0]
    grouped = gated.reshape(length, group_count, -1)
    normed = grouped * lax.rsqrt(jnp.mean(grouped * grouped, axis=-1, keepdims=True) + EPSILON)
    return (normed.reshape(length, -1) * group_gain).astype(jnp.bfloat16)


def chain_step(preceding_entries, later):
    return (
        preceding_entries[0] + later[0],
        jnp.exp(later[0])[:, None, None] * preceding_entries[1] + later[1],
    )


def on_device(
    latent,
    context,
    condition,
    context_condition,
    shift_weight,
    scale_weight,
    gate_weight,
    norm_gain,
    out_gate_weight,
    signal_weight,
    writer_weight,
    reader_matrix,
    step_weight,
    signal_taps,
    writer_taps,
    reader_taps,
    step_bias,
    decay_log,
    decay_extra,
    group_gain,
    output_weight,
):
    rows_here = shift_weight.shape[0]
    cond_act = jax.nn.silu(jnp.stack([condition, context_condition]).astype(jnp.float32)).astype(
        jnp.bfloat16
    )
    own_rows = lax.dynamic_slice_in_dim(cond_act, lax.axis_index("sp") * rows_here, rows_here, 1)
    shift_part = jnp.dot(own_rows, shift_weight, preferred_element_type=jnp.float32)
    scale_part = jnp.dot(own_rows, scale_weight, preferred_element_type=jnp.float32)
    gate_part = jnp.dot(own_rows[:1], gate_weight, preferred_element_type=jnp.float32)
    shift_sum, scale_sum, gate_sum = in_one((shift_part, scale_part, gate_part), "sp")
    shift_vec, scale_vec = side_by_side((shift_sum, scale_sum), ("tp", "dp"), 1, 0)
    gate_vec = gate_sum[0]
    full_rows = lax.all_gather(latent, "dp", axis=0, tiled=True)
    length = full_rows.shape[0]
    hidden = modulate(full_rows, norm_gain, shift_vec[0], scale_vec[0])
    ctx_hidden = modulate(context, norm_gain, shift_vec[1], scale_vec[1])
    conv_taps = jnp.concatenate([signal_taps, writer_taps, reader_taps], axis=1)
    decay_rates = -jnp.exp(decay_log)[:, None, :]
    head_count = step_bias.shape[1]
    head_width = signal_weight.shape[1] // head_count
    group_count = writer_weight.shape[1] // STATE
    per_group = head_count // group_count
    ctx_raw, ctx_step_in = project_rows(
        ctx_hidden, signal_weight, writer_weight, reader_matrix, step_weight
    )
    every_raw, every_step = rows_first((ctx_raw, ctx_step_in), "sp", (0, 1))
    ctx_len = every_raw.shape[0]
    ctx_conv = centred_conv(jnp.pad(every_raw, ((1, 1), (0, 0))), conv_taps, ctx_len)
    ctx_signal, ctx_writer, _ = split_mixed(ctx_conv, head_count, head_width, group_count, STATE)
    prefix_stride_length = jax.nn.softplus(every_step.astype(jnp.float32) + step_bias[:, None, :])
    ctx_decay = decay_rates * prefix_stride_length
    cum_log = jnp.cumsum(ctx_decay, axis=1)
    ctx_forward = context_state(
        ctx_signal, jnp.exp(cum_log[0, -1:] - cum_log[0]) * prefix_stride_length[0], ctx_writer
    )
    ctx_backward = context_state(
        ctx_signal, jnp.exp(cum_log[1] - ctx_decay[1]) * prefix_stride_length[1], ctx_writer
    )
    gate_in = jnp.dot(hidden, out_gate_weight, preferred_element_type=jnp.float32).astype(
        jnp.bfloat16
    )
    raw_cols, step_in = project_rows(
        hidden, signal_weight, writer_weight, reader_matrix, step_weight
    )
    padded = extended(raw_cols, (("sp", 0),), 1)
    signal, writer, reader = split_mixed(
        centred_conv(padded, conv_taps, length), head_count, head_width, group_count, STATE
    )
    step_size = jax.nn.softplus(step_in.astype(jnp.float32) + step_bias[:, None, :])
    log_decay = decay_rates * step_size + jnp.swapaxes(decay_extra, 1, 2)
    zero_state = jnp.zeros((head_count, head_width, STATE), jnp.float32)
    forward_out, forward_last = state_span(
        signal, step_size[0], log_decay[0], writer, reader, zero_state, BLOCK
    )
    back_signal = jnp.flip(signal, 0)
    back_reader = jnp.flip(reader, 0)
    back_decay = jnp.flip(log_decay[1], 0)
    backward_out, backward_last = state_span(
        back_signal,
        jnp.flip(step_size[1], 0),
        back_decay,
        jnp.flip(writer, 0),
        back_reader,
        zero_state,
        BLOCK,
    )
    cum_forward = jnp.cumsum(log_decay[0], axis=0)
    cumulative_backward = jnp.cumsum(back_decay, axis=0)
    identity = (jnp.zeros((head_count,), jnp.float32), zero_state)
    onward_inflow = entering((cum_forward[-1], forward_last), "sp", chain_step, identity, False)
    enter_bwd = entering((cumulative_backward[-1], backward_last), "sp", chain_step, identity, True)
    start_fwd = jnp.exp(onward_inflow[0])[:, None, None] * ctx_forward + onward_inflow[1]
    start_bwd = jnp.exp(enter_bwd[0])[:, None, None] * ctx_backward + enter_bwd[1]
    reader_head_rows = jnp.repeat(reader, per_group, axis=1)
    back_heads = jnp.repeat(back_reader, per_group, axis=1)
    forward_out = (
        forward_out
        + jnp.einsum("thn,hpn->thp", reader_head_rows, start_fwd) * jnp.exp(cum_forward)[..., None]
    )
    backward_out = (
        backward_out
        + jnp.einsum("thn,hpn->thp", back_heads, start_bwd)
        * jnp.exp(cumulative_backward)[..., None]
    )
    both = (forward_out + jnp.flip(backward_out, 0)).reshape(length, -1)
    gated = both * jax.nn.silu(gate_in.astype(jnp.float32))
    normed = group_norm(gated, group_count, group_gain)
    mix = jnp.dot(
        lax.all_gather(normed, ("tp", "dp"), axis=1, tiled=True),
        output_weight,
        preferred_element_type=jnp.float32,
    )
    out_start = lax.axis_index(("tp", "dp")) * output_weight.shape[1]
    residual = lax.dynamic_slice_in_dim(full_rows, out_start, output_weight.shape[1], 1).astype(
        jnp.float32
    )
    return (residual + gate_vec * mix).astype(jnp.bfloat16)


def solution(mesh):
    in_specs = (
        P(("grp", "sp", "dp"), None),
        P(("grp", "sp"), None),
        P("grp"),
        P(),
        P("sp", ("tp", "dp")),
        P("sp", ("tp", "dp")),
        P("sp", ("tp", "dp")),
        P(),
        P(None, ("tp", "dp")),
        P(None, ("tp", "dp")),
        P(None, ("tp", "dp")),
        P(None, ("tp", "dp")),
        P(None, None, ("tp", "dp")),
        P(None, ("tp", "dp")),
        P(None, ("tp", "dp")),
        P(None, ("tp", "dp")),
        P(None, ("tp", "dp")),
        P(None, ("tp", "dp")),
        P(None, ("tp", "dp"), ("grp", "sp")),
        P(("tp", "dp")),
        P(None, ("tp", "dp")),
    )
    out_specs = P(("grp", "sp"), ("tp", "dp"))
    return jax.shard_map(
        on_device, mesh=mesh, in_specs=in_specs, out_specs=out_specs, check_vma=False
    )
```

profile of v0, /device:TPU:33, one launch (start us, length us, event | category | flops | bytes accessed | tf_op | source)
XLA Modules:
  0.0 478.3 jit_solution(13487710746028656442)
XLA Ops:
  8.9 24.5 %all-to-all-start = ((f32[16,1,2560]{2,1,0:T(1,128)}), f32[16,1,2560]{2,1,0:T(1,128)S(1)}, u32[]{:S(2)}, u32[]{:S(2)}) async-start(f32[16,1,2560]{2,1,0:T(1,128)} %broadcast_in_dim.34), calls=%async_computation | async-start | bytes 327680 | tf_op jit(solution)/shard_map/all_to_all | solution.py:13
  34.5 10.9 %all-to-all-done = f32[16,1,2560]{2,1,0:T(1,128)S(1)} async-done(((f32[16,1,2560]{2,1,0:T(1,128)}), f32[16,1,2560]{2,1,0:T(1,128)S(1)}, u32[]{:S(2)}, u32[]{:S(2)}) %all-to-all-start) | async-done | bytes 163872 | tf_op jit(solution)/shard_map/all_to_all | solution.py:13
  45.6 17.6 %all_gather.25 = f32[4,4096]{1,0:T(4,128)S(1)} all-gather(f32[4,512]{1,0:T(4,128)S(1)} %pad_maximum_fusion.9), channel_id=1, replica_groups=mesh['grp'=2,'sp'=16,'tp'=4,'dp'=2] {'tp','dp'}, dimensions={1}, use_global_device_ids=true | all-gather | bytes 73728 | tf_op jit(solution)/shard_map/all_gather | solution.py:35
  67.6 25.9 %all_gather.28 = bf16[512,520]{1,0:T(8,128)(2,1)S(1)} all-gather(bf16[32,520]{1,0:T(8,128)(2,1)S(1)} %pad_maximum_fusion.7), channel_id=1, replica_groups=mesh['grp'=2,'sp'=16,'tp'=4,'dp'=2] {'sp'}, dimensions={0}, use_global_device_ids=true | all-gather | bytes 565760 | tf_op jit(solution)/shard_map/all_gather | solution.py:42
  101.1 4.2 fusion.4
  105.7 3.1 fusion.8
  121.2 4.7 collective-permute-start
  128.5 3.3 rev.19
  161.5 20.6 %all-gather.1 = f32[16,1,4]{2,1,0:T(1,128)} all-gather(f32[1,1,4]{2,1,0:T(1,128)} %bitcast.351), channel_id=1, replica_groups=mesh['grp'=2,'sp'=16,'tp'=4,'dp'=2] {'sp'}, dimensions={0}, use_global_device_ids=true | all-gather | bytes 272 | tf_op jit(solution)/shard_map/all_gather | solution.py:71
  182.1 21.8 %all-gather = f32[16,1,4]{2,1,0:T(1,128)} all-gather(f32[1,1,4]{2,1,0:T(1,128)} %bitcast.352), channel_id=1, replica_groups=mesh['grp'=2,'sp'=16,'tp'=4,'dp'=2] {'sp'}, dimensions={0}, use_global_device_ids=true | all-gather | bytes 272 | tf_op jit(solution)/shard_map/all_gather | solution.py:71
  204.0 4.9 %divide_multiply_fusion = f32[768,512]{0,1:T(8,128)S(1)} fusion(bf16[1,512]{0,1:T(8,128)(2,1)S(1)} %collective-permute-done.1, bf16[768,128]{0,1:T(8,128)(2,1)S(1)} %copy-done.15, bf16[768,128]{0,1:T(8,128)(2,1)S(1)} %copy-done.17, bf16[768,256]{0,1:T(8,128)(2,1)} %copy-done.23, bf16[1,512]{0,1:T(8,128)(2,1)} %collective-permute-done, f32[512]{0:T(512)} %bitcast.339, ...), kind=kLoop, calls=%fused_computation.35 | loop fusion | flops 12189696 | bytes 2367488 | tf_op jit(solution)/shard_map/jit(silu)/mul | solution.py:97
  209.8 3.8 reverse.6
  215.3 3.8 reverse.7
  232.5 8.2 %while.62 = (s32[]{:T(128)}, f32[1,4,64,128]{3,2,1,0:T(8,128)S(1)}, bf16[6,1,4,64,128]{4,3,2,1,0:T(8,128)(2,1)}, f32[6,1,4]{2,1,0:T(1,128)}, f32[6,1,4,64,128]{4,3,2,1,0:T(8,128)S(1)}, /*index=5*/s32[]{:T(128)}, s32[]{:T(128)}) while((s32[]{:T(128)}, f32[1,4,64,128]{3,2,1,0:T(8,128)S(1)}, ...), condition=%wide.region_14.15_spmd.clone, body=%wide.region_13.14_spmd.clone.sunk | while | flops 131075 | bytes 589980 | solution.py:153
  253.6 10.1 %while.60 = (s32[]{:T(128)}, f32[1,4,64,128]{3,2,1,0:T(8,128)S(1)}, bf16[6,1,4,64,128]{4,3,2,1,0:T(8,128)(2,1)S(1)}, f32[6,1,4]{2,1,0:T(1,128)}, f32[6,1,4,64,128]{4,3,2,1,0:T(8,128)}, /*index=5*/s32[]{:T(128)}, s32[]{:T(128)}) while((s32[]{:T(128)}, f32[1,4,64,128]{3,2,1,0:T(8,128)S(1)}, ...), condition=%wide.region_4.5_spmd.clone, body=%wide.region_3.4_spmd.clone.sunk | while | flops 131075 | bytes 589980 | solution.py:153
  266.9 52.0 %all-gather.11.cloned.1.call-done = f32[16,4,64,128]{3,2,1,0:T(8,128)} async-done(((f32[1,4,64,128]{3,2,1,0:T(8,128)}), f32[16,4,64,128]{3,2,1,0:T(8,128)}) %all-gather.11.cloned.1.call-update) | async-done | bytes 2097168 | tf_op jit(solution)/shard_map/all_gather | solution.py:71
  318.9 27.4 %while.63 = (s32[]{:T(128)}, f32[4]{0:T(128)S(1)}, f32[4,64,128]{2,1,0:T(8,128)S(1)}, s32[]{:T(128)}, f32[16,4]{1,0:T(8,128)}, /*index=5*/f32[16,4,64,128]{3,2,1...) while((s32[]{:T(128)}, f32[4]{0:T(128)S(1)}, f32[4,64,128]{2,1,0:T(8,128)S(1)}, ...), condition=%wide.region_18.19_spmd.clone, body=%wide.region_17.18_spmd.clone.sunk | while | flops 131092 | bytes 393481 | solution.py:82
  349.1 4.5 rev.20
  353.6 35.5 %all-gather.9.cloned.1.call-done = f32[16,4,64,128]{3,2,1,0:T(8,128)} async-done(((f32[1,4,64,128]{3,2,1,0:T(8,128)}), f32[16,4,64,128]{3,2,1,0:T(8,128)}) %all-gather.9.cloned.1.call-update) | async-done | bytes 2097168 | tf_op jit(solution)/shard_map/all_gather | solution.py:71
  389.1 27.4 %while.61 = (s32[]{:T(128)}, f32[4]{0:T(128)S(1)}, f32[4,64,128]{2,1,0:T(8,128)S(1)}, s32[]{:T(128)}, f32[16,4]{1,0:T(8,128)}, /*index=5*/f32[16,4,64,128]{3,2,1,0:T(8,128)}, s32[]{:T(128)}, s32[]{:T(128)}) while((s32[]{:T(128)}, f32[4]{0:T(128)S(1)}, f32[4,64,128]{2,1,0:T(8,128)S(1)}, s32[]{:T(128)}, f32[16,4]{1,0:T(8,128)}, ...), condition=%wide.region_8.9_spmd.clone, body=%wide.region_7.8_spmd.clone.sunk | while | flops 131088 | bytes 393419 | solution.py:82
  416.5 2.9 fusion.27
  419.4 5.5 %multiply_reduce_fusion = (f32[768]{0:T(1024)S(1)}, f32[768,256]{0,1:T(8,128)S(1)}) fusion(bf16[768,4096]{1,0:T(8,128)(2,1)} %copy-done.1, bf16[4096,256]{1,0:T(8,128)(2,1)} %param.37, f32[768,4,64]{0,2,1:T(8,128)} %fusion.27), kind=kOutput, calls=%fused_computation.95 | convolution fusion | flops 1612381440 | bytes 9964544 | tf_op jit(solution)/shard_map/dot_general | solution.py:247
  425.9 41.1 %all-gather.13.cloned.1.call-done = bf16[768,2048]{0,1:T(8,128)(2,1)} async-done(((bf16[768,256]{0,1:T(8,128)(2,1)}), bf16[768,2048]{0,1:T(8,128)(2,1)}) %all-gather.13.cloned.1.call-update) | async-done | bytes 3145744 | tf_op jit(solution)/shard_map/all_gather | solution.py:297
  467.0 4.8 add_convert_fusion
  (364 shorter events, 167.6 us)
Async XLA Ops:
  6.5 460.5 %copy-start = (bf16[2048,512]{1,0:T(8,128)(2,1)S(1)}, bf16[2048,512]{1,0:T(8,128)(2,1)}, u32[]{:S(2)}) copy-start(bf16[2048,512]{1,0:T(8,128)(2,1)} %param.49) | copy-start | bytes 6291460
  6.6 94.5 %all-gather.7.cloned.1.call-start = ((), (), s32[]{:S(2)}) async-start(), calls=%async_computation.1 | async-start | bytes 9437184 | tf_op jit(solution)/shard_map/all_gather | solution.py:221
  7.4 55.8 %copy-start.31 = (f32[4096]{0:T(1024)S(1)}, f32[4096]{0:T(1024)}, u32[]{:S(2)}) copy-start(f32[4096]{0:T(1024)} %param.36) | copy-start | bytes 49156
  7.4 56.0 %copy-start.28 = (bf16[2,4096,4]{1,2,0:T(4,128)(2,1)S(1)}, bf16[2,4096,4]{1,2,0:T(4,128)(2,1)}, u32[]{:S(2)}) copy-start(bf16[2,4096,4]{1,2,0:T(4,128)(2,1)} %param.41) | copy-start | bytes 196612
  8.9 36.5 %all-to-all-start = ((f32[16,1,2560]{2,1,0:T(1,128)}), f32[16,1,2560]{2,1,0:T(1,128)S(1)}, u32[]{:S(2)}, u32[]{:S(2)}) async-start(f32[16,1,2560]{2,1,0:T(1,128)} %broadcast_in_dim.34), calls=%async_computation | async-start | bytes 327680 | tf_op jit(solution)/shard_map/all_to_all | solution.py:13
  33.4 285.4 %all-gather.11.cloned.1.call-start = ((), (), s32[]{:S(2)}) async-start(), calls=%async_computation.3 | async-start | bytes 2228224 | tf_op jit(solution)/shard_map/all_gather | solution.py:71
  34.4 59.1 %copy-start.41 = (f32[1,512]{1,0:T(1,128)}, f32[1,512]{1,0:T(1,128)S(1)}, u32[]{:S(2)}) copy-start(f32[1,512]{1,0:T(1,128)S(1)} %get-tuple-element.663) | copy-start | bytes 6148
  34.5 59.1 %copy-start.42 = (f32[1,512]{1,0:T(1,128)}, f32[1,512]{1,0:T(1,128)S(1)}, u32[]{:S(2)}) copy-start(f32[1,512]{1,0:T(1,128)S(1)} %get-tuple-element.664) | copy-start | bytes 6148
  34.5 59.1 %copy-start.43 = (f32[1,512]{1,0:T(1,128)}, f32[1,512]{1,0:T(1,128)S(1)}, u32[]{:S(2)}) copy-start(f32[1,512]{1,0:T(1,128)S(1)} %get-tuple-element.665) | copy-start | bytes 6148
  119.9 84.0 %collective-permute-start.1 = (bf16[1,512]{0,1:T(8,128)(2,1)}, bf16[1,512]{0,1:T(8,128)(2,1)S(1)}, u32[]{:S(2)}, u32[]{:S(2)}) collective-permute-start(bf16[1,512]{0,1:T(8,128)(2,1)} %get-tuple-element.645), channel_id=1, source_target_pairs={{8,0},{16,8},{24,16},{32,24},{40,32},{48,40},{56,48},{64,56},{72,6... | collective-permute-start | bytes 3080 | tf_op jit(solution)/shard_map/ppermute | solution.py:62
  121.2 82.7 %collective-permute-start = (bf16[1,512]{0,1:T(8,128)(2,1)}, bf16[1,512]{0,1:T(8,128)(2,1)}, u32[]{:S(2)}, u32[]{:S(2)}) collective-permute-start(bf16[1,512]{0,1:T(8,128)(2,1)} %get-tuple-element.644), channel_id=1, source_target_pairs={{0,8},{8,16},{16,24},{24,32},{32,40},{40,48},{48,56},{56,64},{64,7... | collective-permute-start | bytes 3080 | tf_op jit(solution)/shard_map/ppermute | solution.py:60
  150.0 53.9 %copy-start.15 = (bf16[768,128]{0,1:T(8,128)(2,1)S(1)}, bf16[768,128]{0,1:T(8,128)(2,1)}, u32[]{:S(2)}) copy-start(bf16[768,128]{0,1:T(8,128)(2,1)} %copy-done.14) | copy-start | bytes 589828
  150.0 53.9 %copy-start.17 = (bf16[768,128]{0,1:T(8,128)(2,1)S(1)}, bf16[768,128]{0,1:T(8,128)(2,1)}, u32[]{:S(2)}) copy-start(bf16[768,128]{0,1:T(8,128)(2,1)} %copy-done.16) | copy-start | bytes 589828
  241.5 147.6 %all-gather.9.cloned.1.call-start = ((), (), s32[]{:S(2)}) async-start(), calls=%async_computation.2 | async-start | bytes 2228224 | tf_op jit(solution)/shard_map/all_gather | solution.py:71
  265.2 53.7 %copy-start.46 = (f32[4]{0:T(128)S(1)}, f32[4]{0:T(128)}, u32[]{:S(2)}) copy-start(f32[4]{0:T(128)} %custom-call.4) | copy-start | bytes 52
  266.8 79.6 %copy-start.5 = (f32[512,256]{0,1:T(8,128)S(1)}, f32[512,256]{0,1:T(8,128)}, u32[]{:S(2)}) copy-start(f32[512,256]{0,1:T(8,128)} %copy.318) | copy-start | bytes 1572868
  266.8 79.6 %copy-start.36 = (f32[768,4]{0,1:T(4,128)S(1)}, f32[768,4]{0,1:T(4,128)}, u32[]{:S(2)}) copy-start(f32[768,4]{0,1:T(4,128)} %get-tuple-element.636) | copy-start | bytes 36868
  266.8 79.6 %copy-start.39 = (f32[512,4]{0,1:T(4,128)S(1)}, f32[512,4]{0,1:T(4,128)}, u32[]{:S(2)}) copy-start(f32[512,4]{0,1:T(4,128)} %fusion.94) | copy-start | bytes 24580
  266.8 200.2 %all-gather.13.cloned.1.call-start = ((), (), s32[]{:S(2)}) async-start(), calls=%async_computation.4 | async-start | bytes 3538944 | tf_op jit(solution)/shard_map/all_gather | solution.py:297
  346.4 42.7 %copy-start.45 = (f32[4]{0:T(128)S(1)}, f32[4]{0:T(128)}, u32[]{:S(2)}) copy-start(f32[4]{0:T(128)} %custom-call.1) | copy-start | bytes 52
  349.1 67.4 %copy-start.12 = (bf16[768,128]{1,0:T(8,128)(2,1)S(1)}, bf16[768,128]{1,0:T(8,128)(2,1)}, u32[]{:S(2)}) copy-start(bf16[768,128]{1,0:T(8,128)(2,1)} %copy.303) | copy-start | bytes 589828
  349.1 67.4 %copy-start.35 = (f32[768,4]{0,1:T(4,128)S(1)}, f32[768,4]{0,1:T(4,128)}, u32[]{:S(2)}) copy-start(f32[768,4]{0,1:T(4,128)} %get-tuple-element.632) | copy-start | bytes 36868
  349.1 67.4 %copy-start.38 = (f32[512,4]{0,1:T(4,128)S(1)}, f32[512,4]{0,1:T(4,128)}, u32[]{:S(2)}) copy-start(f32[512,4]{0,1:T(4,128)} %fusion.95) | copy-start | bytes 24580
  424.9 42.1 %slice-start = ((f32[2560]{0:T(1024)}), f32[512]{0:T(512)S(1)}, s32[]{:S(2)}) async-start(f32[2560]{0:T(1024)} %copy-done.37), calls=%async_computation.5 | async-start | bytes 4096 | tf_op jit(solution)/shard_map/slice | solution.py:26
  (40 other events, 267.3 us)
Sparse Core Ops, SparseCore 0:
  9.3 41.3 all-gather.6
  241.6 77.2 all-gather.10
  320.7 68.3 all-gather.8
  426.0 40.9 all-gather.12
where the time goes:
time: 482 us; the launch traced here: 478 us
  waiting for transfers between devices  140 us (29%)
  other arithmetic  98.2 us (20%)
  blocking collectives  85.9 us (18%)
  local copies, waits for them, and re-layouts  67.5 us (14%)
  matrix products  40.4 us (8%)
  starting transfers between devices  30.8 us (6%)
  between operations  14.2 us (3%)
    all_gather x2, waiting for transfers between devices, entering(): everything = jax.tree.map(lambda part: lax.all_gather(part, axis), x)  87.5 us
    all_gather x2, blocking collectives, entering(): everything = jax.tree.map(lambda part: lax.all_gather(part, axis), x)  42.4 us
    all_gather x1, waiting for transfers between devices, on_device(): lax.all_gather(normed, ('tp', 'dp'), axis=1, tiled=True)  41.1 us
    select_n x32, other arithmetic, turn(): return jax.tree.map(lambda a, b: jnp.where(reached, a, b), new, before)  31.6 us
    all_gather x1, blocking collectives, rows_first(): out = lax.all_gather(both, axis, axis=0, tiled=True)  25.9 us
    all_to_all x1, starting transfers between devices, copy_for_each(): return lax.all_to_all(copies, axis, split_axis=0, concat_axis=0, tiled=True)  24.5 us
    exp x32, other arithmetic, chain_step(): jnp.exp(later[0])[:, None, None] * preceding_entries[1] + later[1]  22.3 us
    all_gather x1, blocking collectives, side_by_side(): lax.all_gather(both, axis, axis=dim, tiled=True)  17.6 us
  transfers between devices with their start and end apart: 7, of which 4 were waited for; matrix products, arithmetic and copies ran while one was open for 22% of the time, Pallas kernels for 0%

commit v1 on v0

--- a/solution.py
+++ b/solution.py
@@ -294,7 +294,10 @@
     gated = both * jax.nn.silu(gate_in.astype(jnp.float32))
     normed = group_norm(gated, group_count, group_gain)
     mix = jnp.dot(
-        lax.all_gather(normed, ("tp", "dp"), axis=1, tiled=True),
+        jnp.concatenate(
+            lax.all_to_all(jnp.stack([normed] * lax.axis_size(("tp", "dp"))), ("tp", "dp"), 0, 0),
+            axis=1,
+        ),
         output_weight,
         preferred_element_type=jnp.float32,
     )

time: 482 us -> 494 us (1.025)
  starting transfers between devices: 30.8 us -> 45.5 us
    all_gather x1 -> x0, waiting for transfers between devices: 41.1 us -> none  [on_device(): lax.all_gather(normed, ('tp', 'dp'), axis=1, tiled=True)]
    all_to_all x0 -> x1, waiting for transfers between devices: none -> 37.6 us  [on_device(): lax.all_to_all(jnp.stack([normed] * lax.axis_size(('tp', 'dp'))), ('tp',...]
    all_to_all x0 -> x1, starting transfers between devices: none -> 14.8 us  [on_device(): lax.all_to_all(jnp.stack([normed] * lax.axis_size(('tp', 'dp'))), ('tp',...]
    another operation x12 -> x13, local copies, waits for them, and re-layouts: 13.4 us -> 15.3 us
where the time goes in v1:
time: 494 us; the launch traced here: 490 us
  waiting for transfers between devices  136 us (28%)
  other arithmetic  97.2 us (20%)
  blocking collectives  86.1 us (17%)
  local copies, waits for them, and re-layouts  69.4 us (14%)
  starting transfers between devices  45.5 us (9%)
  matrix products  40.4 us (8%)
  between operations  14.1 us (3%)
    all_gather x2, waiting for transfers between devices, entering(): everything = jax.tree.map(lambda part: lax.all_gather(part, axis), x)  87 us
    all_gather x2, blocking collectives, entering(): everything = jax.tree.map(lambda part: lax.all_gather(part, axis), x)  42.6 us
    all_to_all x1, waiting for transfers between devices, on_device(): lax.all_to_all(jnp.stack([normed] * lax.axis_size(('tp', 'dp'))), ('tp',...  37.6 us
    select_n x32, other arithmetic, turn(): return jax.tree.map(lambda a, b: jnp.where(reached, a, b), new, before)  31.6 us
    all_gather x1, blocking collectives, rows_first(): out = lax.all_gather(both, axis, axis=0, tiled=True)  25.9 us
    all_to_all x1, starting transfers between devices, copy_for_each(): return lax.all_to_all(copies, axis, split_axis=0, concat_axis=0, tiled=True)  24.5 us
    exp x32, other arithmetic, chain_step(): jnp.exp(later[0])[:, None, None] * preceding_entries[1] + later[1]  22.2 us
    all_gather x1, blocking collectives, side_by_side(): lax.all_gather(both, axis, axis=dim, tiled=True)  17.6 us
  transfers between devices with their start and end apart: 7, of which 4 were waited for; matrix products, arithmetic and copies ran while one was open for 22% of the time, Pallas kernels for 0%

profile of v1, /device:TPU:33, one launch (start us, length us, event | category | flops | bytes accessed | tf_op | source)
XLA Modules:
  0.0 490.4 jit_solution(4143906756519044354)
XLA Ops:
  8.9 24.5 %all-to-all-start = ((f32[16,1,2560]{2,1,0:T(1,128)}), f32[16,1,2560]{2,1,0:T(1,128)S(1)}, u32[]{:S(2)}, u32[]{:S(2)}) async-start(f32[16,1,2560]{2,1,0:T(1,128)} %broadcast_in_dim.34), calls=%async_computation | async-start | bytes 327680 | tf_op jit(solution)/shard_map/all_to_all | solution.py:13
  34.5 10.9 %all-to-all-done = f32[16,1,2560]{2,1,0:T(1,128)S(1)} async-done(((f32[16,1,2560]{2,1,0:T(1,128)}), f32[16,1,2560]{2,1,0:T(1,128)S(1)}, u32[]{:S(2)}, u32[]{:S(2)}) %all-to-all-start) | async-done | bytes 163872 | tf_op jit(solution)/shard_map/all_to_all | solution.py:13
  45.6 17.6 %all_gather.22 = f32[4,4096]{1,0:T(4,128)S(1)} all-gather(f32[4,512]{1,0:T(4,128)S(1)} %pad_maximum_fusion.9), channel_id=1, replica_groups=mesh['grp'=2,'sp'=16,'tp'=4,'dp'=2] {'tp','dp'}, dimensions={1}, use_global_device_ids=true | all-gather | bytes 73728 | tf_op jit(solution)/shard_map/all_gather | solution.py:35
  67.6 25.9 %all_gather.25 = bf16[512,520]{1,0:T(8,128)(2,1)S(1)} all-gather(bf16[32,520]{1,0:T(8,128)(2,1)S(1)} %pad_maximum_fusion.7), channel_id=1, replica_groups=mesh['grp'=2,'sp'=16,'tp'=4,'dp'=2] {'sp'}, dimensions={0}, use_global_device_ids=true | all-gather | bytes 565760 | tf_op jit(solution)/shard_map/all_gather | solution.py:42
  101.1 4.2 fusion.4
  105.7 3.1 fusion.8
  121.2 4.7 collective-permute-start
  128.4 3.3 rev.19
  161.4 20.4 %all-gather.1 = f32[16,1,4]{2,1,0:T(1,128)} all-gather(f32[1,1,4]{2,1,0:T(1,128)} %bitcast.354), channel_id=1, replica_groups=mesh['grp'=2,'sp'=16,'tp'=4,'dp'=2] {'sp'}, dimensions={0}, use_global_device_ids=true | all-gather | bytes 272 | tf_op jit(solution)/shard_map/all_gather | solution.py:71
  181.8 22.1 %all-gather = f32[16,1,4]{2,1,0:T(1,128)} all-gather(f32[1,1,4]{2,1,0:T(1,128)} %bitcast.355), channel_id=1, replica_groups=mesh['grp'=2,'sp'=16,'tp'=4,'dp'=2] {'sp'}, dimensions={0}, use_global_device_ids=true | all-gather | bytes 272 | tf_op jit(solution)/shard_map/all_gather | solution.py:71
  204.0 4.9 %divide_multiply_fusion = f32[768,512]{0,1:T(8,128)S(1)} fusion(bf16[1,512]{0,1:T(8,128)(2,1)S(1)} %collective-permute-done.1, bf16[768,128]{0,1:T(8,128)(2,1)S(1)} %copy-done.15, bf16[768,128]{0,1:T(8,128)(2,1)S(1)} %copy-done.17, bf16[768,256]{0,1:T(8,128)(2,1)} %copy-done.23, bf16[1,512]{0,1:T(8,128)(2,1)} %collective-permute-done, f32[512]{0:T(512)} %bitcast.342, ...), kind=kLoop, calls=%fused_computation.35 | loop fusion | flops 12189696 | bytes 2367488 | tf_op jit(solution)/shard_map/jit(silu)/mul | solution.py:97
  209.8 3.8 reverse.6
  215.3 3.8 reverse.7
  232.6 8.3 %while.62 = (s32[]{:T(128)}, f32[1,4,64,128]{3,2,1,0:T(8,128)S(1)}, bf16[6,1,4,64,128]{4,3,2,1,0:T(8,128)(2,1)}, f32[6,1,4]{2,1,0:T(1,128)}, f32[6,1,4,64,128]{4,3,2,1,0:T(8,128)S(1)}, /*index=5*/s32[]{:T(128)}, s32[]{:T(128)}) while((s32[]{:T(128)}, f32[1,4,64,128]{3,2,1,0:T(8,128)S(1)}, ...), condition=%wide.region_14.15_spmd.clone, body=%wide.region_13.14_spmd.clone.sunk | while | flops 131075 | bytes 589980 | solution.py:153
  253.8 10.3 %while.60 = (s32[]{:T(128)}, f32[1,4,64,128]{3,2,1,0:T(8,128)S(1)}, bf16[6,1,4,64,128]{4,3,2,1,0:T(8,128)(2,1)S(1)}, f32[6,1,4]{2,1,0:T(1,128)}, f32[6,1,4,64,128]{4,3,2,1,0:T(8,128)}, /*index=5*/s32[]{:T(128)}, s32[]{:T(128)}) while((s32[]{:T(128)}, f32[1,4,64,128]{3,2,1,0:T(8,128)S(1)}, ...), condition=%wide.region_4.5_spmd.clone, body=%wide.region_3.4_spmd.clone.sunk | while | flops 131075 | bytes 589980 | solution.py:153
  267.2 51.8 %all-gather.10.cloned.1.call-done = f32[16,4,64,128]{3,2,1,0:T(8,128)} async-done(((f32[1,4,64,128]{3,2,1,0:T(8,128)}), f32[16,4,64,128]{3,2,1,0:T(8,128)}) %all-gather.10.cloned.1.call-update) | async-done | bytes 2097168 | tf_op jit(solution)/shard_map/all_gather | solution.py:71
  319.0 27.4 %while.63 = (s32[]{:T(128)}, f32[4]{0:T(128)S(1)}, f32[4,64,128]{2,1,0:T(8,128)S(1)}, s32[]{:T(128)}, f32[16,4]{1,0:T(8,128)}, /*index=5*/f32[16,4,64,128]{3,2,1...) while((s32[]{:T(128)}, f32[4]{0:T(128)S(1)}, f32[4,64,128]{2,1,0:T(8,128)S(1)}, ...), condition=%wide.region_18.19_spmd.clone, body=%wide.region_17.18_spmd.clone.sunk | while | flops 131092 | bytes 393481 | solution.py:82
  349.2 4.5 rev.20
  353.7 35.2 %all-gather.8.cloned.1.call-done = f32[16,4,64,128]{3,2,1,0:T(8,128)} async-done(((f32[1,4,64,128]{3,2,1,0:T(8,128)}), f32[16,4,64,128]{3,2,1,0:T(8,128)}) %all-gather.8.cloned.1.call-update) | async-done | bytes 2097168 | tf_op jit(solution)/shard_map/all_gather | solution.py:71
  388.9 27.3 %while.61 = (s32[]{:T(128)}, f32[4]{0:T(128)S(1)}, f32[4,64,128]{2,1,0:T(8,128)S(1)}, s32[]{:T(128)}, f32[16,4]{1,0:T(8,128)}, /*index=5*/f32[16,4,64,128]{3,2,1,0:T(8,128)}, s32[]{:T(128)}, s32[]{:T(128)}) while((s32[]{:T(128)}, f32[4]{0:T(128)S(1)}, f32[4,64,128]{2,1,0:T(8,128)S(1)}, s32[]{:T(128)}, f32[16,4]{1,0:T(8,128)}, ...), condition=%wide.region_8.9_spmd.clone, body=%wide.region_7.8_spmd.clone.sunk | while | flops 131088 | bytes 393419 | solution.py:82
  419.1 5.5 %multiply_reduce_fusion = (f32[768]{0:T(1024)S(1)}, f32[768,256]{0,1:T(8,128)S(1)}) fusion(bf16[768,4096]{1,0:T(8,128)(2,1)} %copy-done.1, bf16[4096,256]{1,0:T(8,128)(2,1)} %param.37, f32[768,4,64]{0,2,1:T(8,128)} %fusion.27), kind=kOutput, calls=%fused_computation.95 | convolution fusion | flops 1612381440 | bytes 9964544 | tf_op jit(solution)/shard_map/dot_general | solution.py:247
  426.6 14.8 %all-to-all-start.1 = ((bf16[8,768,256]{1,2,0:T(8,128)(2,1)}), bf16[8,768,256]{1,2,0:T(8,128)(2,1)}, u32[]{:S(2)}, u32[]{:S(2)}) async-start(bf16[8,768,256]{1,2,0:T(8,128)(2,1)} %stack.53), calls=%async_computation.1 | async-start | bytes 6291456 | tf_op jit(solution)/shard_map/all_to_all | solution.py:298
  441.4 37.6 %all-to-all-done.1 = bf16[8,768,256]{1,2,0:T(8,128)(2,1)} async-done(((bf16[8,768,256]{1,2,0:T(8,128)(2,1)}), bf16[8,768,256]{1,2,0:T(8,128)(2,1)}, u32[]{:S(2)}, u32[]{:S(2)}) %all-to-all-start.1) | async-done | bytes 3145760 | tf_op jit(solution)/shard_map/all_to_all | solution.py:298
  479.1 4.8 add_convert_fusion
  (364 shorter events, 171.3 us)
Async XLA Ops:
  6.5 472.5 %copy-start = (bf16[2048,512]{1,0:T(8,128)(2,1)S(1)}, bf16[2048,512]{1,0:T(8,128)(2,1)}, u32[]{:S(2)}) copy-start(bf16[2048,512]{1,0:T(8,128)(2,1)} %param.49) | copy-start | bytes 6291460
  6.6 94.5 %all-gather.6.cloned.1.call-start = ((), (), s32[]{:S(2)}) async-start(), calls=%async_computation.2 | async-start | bytes 9437184 | tf_op jit(solution)/shard_map/all_gather | solution.py:221
  7.4 55.8 %copy-start.31 = (f32[4096]{0:T(1024)S(1)}, f32[4096]{0:T(1024)}, u32[]{:S(2)}) copy-start(f32[4096]{0:T(1024)} %param.36) | copy-start | bytes 49156
  7.4 56.0 %copy-start.28 = (bf16[2,4096,4]{1,2,0:T(4,128)(2,1)S(1)}, bf16[2,4096,4]{1,2,0:T(4,128)(2,1)}, u32[]{:S(2)}) copy-start(bf16[2,4096,4]{1,2,0:T(4,128)(2,1)} %param.41) | copy-start | bytes 196612
  8.9 36.5 %all-to-all-start = ((f32[16,1,2560]{2,1,0:T(1,128)}), f32[16,1,2560]{2,1,0:T(1,128)S(1)}, u32[]{:S(2)}, u32[]{:S(2)}) async-start(f32[16,1,2560]{2,1,0:T(1,128)} %broadcast_in_dim.34), calls=%async_computation | async-start | bytes 327680 | tf_op jit(solution)/shard_map/all_to_all | solution.py:13
  33.4 285.6 %all-gather.10.cloned.1.call-start = ((), (), s32[]{:S(2)}) async-start(), calls=%async_computation.4 | async-start | bytes 2228224 | tf_op jit(solution)/shard_map/all_gather | solution.py:71
  34.4 59.1 %copy-start.41 = (f32[1,512]{1,0:T(1,128)}, f32[1,512]{1,0:T(1,128)S(1)}, u32[]{:S(2)}) copy-start(f32[1,512]{1,0:T(1,128)S(1)} %get-tuple-element.663) | copy-start | bytes 6148
  34.5 59.1 %copy-start.42 = (f32[1,512]{1,0:T(1,128)}, f32[1,512]{1,0:T(1,128)S(1)}, u32[]{:S(2)}) copy-start(f32[1,512]{1,0:T(1,128)S(1)} %get-tuple-element.664) | copy-start | bytes 6148
  34.5 59.1 %copy-start.43 = (f32[1,512]{1,0:T(1,128)}, f32[1,512]{1,0:T(1,128)S(1)}, u32[]{:S(2)}) copy-start(f32[1,512]{1,0:T(1,128)S(1)} %get-tuple-element.665) | copy-start | bytes 6148
  119.9 84.0 %collective-permute-start.1 = (bf16[1,512]{0,1:T(8,128)(2,1)}, bf16[1,512]{0,1:T(8,128)(2,1)S(1)}, u32[]{:S(2)}, u32[]{:S(2)}) collective-permute-start(bf16[1,512]{0,1:T(8,128)(2,1)} %get-tuple-element.645), channel_id=1, source_target_pairs={{8,0},{16,8},{24,16},{32,24},{40,32},{48,40},{56,48},{64,56},{72,6... | collective-permute-start | bytes 3080 | tf_op jit(solution)/shard_map/ppermute | solution.py:62
  121.2 82.7 %collective-permute-start = (bf16[1,512]{0,1:T(8,128)(2,1)}, bf16[1,512]{0,1:T(8,128)(2,1)}, u32[]{:S(2)}, u32[]{:S(2)}) collective-permute-start(bf16[1,512]{0,1:T(8,128)(2,1)} %get-tuple-element.644), channel_id=1, source_target_pairs={{0,8},{8,16},{16,24},{24,32},{32,40},{40,48},{48,56},{56,64},{64,7... | collective-permute-start | bytes 3080 | tf_op jit(solution)/shard_map/ppermute | solution.py:60
  149.8 54.2 %copy-start.15 = (bf16[768,128]{0,1:T(8,128)(2,1)S(1)}, bf16[768,128]{0,1:T(8,128)(2,1)}, u32[]{:S(2)}) copy-start(bf16[768,128]{0,1:T(8,128)(2,1)} %copy-done.14) | copy-start | bytes 589828
  149.8 54.2 %copy-start.17 = (bf16[768,128]{0,1:T(8,128)(2,1)S(1)}, bf16[768,128]{0,1:T(8,128)(2,1)}, u32[]{:S(2)}) copy-start(bf16[768,128]{0,1:T(8,128)(2,1)} %copy-done.16) | copy-start | bytes 589828
  241.7 147.2 %all-gather.8.cloned.1.call-start = ((), (), s32[]{:S(2)}) async-start(), calls=%async_computation.3 | async-start | bytes 2228224 | tf_op jit(solution)/shard_map/all_gather | solution.py:71
  265.5 53.5 %copy-start.46 = (f32[4]{0:T(128)S(1)}, f32[4]{0:T(128)}, u32[]{:S(2)}) copy-start(f32[4]{0:T(128)} %custom-call.4) | copy-start | bytes 52
  267.1 79.3 %copy-start.5 = (f32[512,256]{0,1:T(8,128)S(1)}, f32[512,256]{0,1:T(8,128)}, u32[]{:S(2)}) copy-start(f32[512,256]{0,1:T(8,128)} %copy.319) | copy-start | bytes 1572868
  267.1 79.3 %copy-start.36 = (f32[768,4]{0,1:T(4,128)S(1)}, f32[768,4]{0,1:T(4,128)}, u32[]{:S(2)}) copy-start(f32[768,4]{0,1:T(4,128)} %get-tuple-element.636) | copy-start | bytes 36868
  267.1 79.3 %copy-start.39 = (f32[512,4]{0,1:T(4,128)S(1)}, f32[512,4]{0,1:T(4,128)}, u32[]{:S(2)}) copy-start(f32[512,4]{0,1:T(4,128)} %fusion.94) | copy-start | bytes 24580
  346.5 42.4 %copy-start.45 = (f32[4]{0:T(128)S(1)}, f32[4]{0:T(128)}, u32[]{:S(2)}) copy-start(f32[4]{0:T(128)} %custom-call.1) | copy-start | bytes 52
  349.2 67.0 %copy-start.12 = (bf16[768,128]{1,0:T(8,128)(2,1)S(1)}, bf16[768,128]{1,0:T(8,128)(2,1)}, u32[]{:S(2)}) copy-start(bf16[768,128]{1,0:T(8,128)(2,1)} %copy.304) | copy-start | bytes 589828
  349.2 67.0 %copy-start.35 = (f32[768,4]{0,1:T(4,128)S(1)}, f32[768,4]{0,1:T(4,128)}, u32[]{:S(2)}) copy-start(f32[768,4]{0,1:T(4,128)} %get-tuple-element.632) | copy-start | bytes 36868
  349.2 67.0 %copy-start.38 = (f32[512,4]{0,1:T(4,128)S(1)}, f32[512,4]{0,1:T(4,128)}, u32[]{:S(2)}) copy-start(f32[512,4]{0,1:T(4,128)} %fusion.95) | copy-start | bytes 24580
  426.6 52.5 %slice-start = ((f32[2560]{0:T(1024)}), f32[512]{0:T(512)S(1)}, s32[]{:S(2)}) async-start(f32[2560]{0:T(1024)} %copy-done.37), calls=%async_computation.5 | async-start | bytes 4096 | tf_op jit(solution)/shard_map/slice | solution.py:26
  426.6 52.4 %all-to-all-start.1 = ((bf16[8,768,256]{1,2,0:T(8,128)(2,1)}), bf16[8,768,256]{1,2,0:T(8,128)(2,1)}, u32[]{:S(2)}, u32[]{:S(2)}) async-start(bf16[8,768,256]{1,2,0:T(8,128)(2,1)} %stack.53), calls=%async_computation.1 | async-start | bytes 6291456 | tf_op jit(solution)/shard_map/all_to_all | solution.py:298
  (40 other events, 267.6 us)
Sparse Core Ops, SparseCore 0:
  9.3 41.3 all-gather.5
  241.8 77.1 all-gather.9
  320.8 68.0 all-gather.7
